TPU v7x, 32 devices: a whole 2x2x4 slice. The times are simulated.
32 devices in a mesh: dp: 4 (over y, x), kv: 4 (over z), tp: 2 (over core).
Axes of the slice: x: 2, y: 2, z: 4, core: 2. Of those that a mesh axis runs over, the one named last changes fastest.
Arguments:
- incoming_vectors: bfloat16 [64, 4096], P('dp', ('kv', 'tp')), may hold values from -36 to 36
- mixer_scaling_vector: float32 [4096], P(('kv', 'tp')), may hold values from 0.1 to 1.9
- probe_matrix: bfloat16 [4096, 2048], P('kv', 'tp'), may hold values from -0.09375 to 0.09375
- address_matrix: bfloat16 [4096, 2048], P('kv', 'tp'), may hold values from -0.09375 to 0.09375
- content_matrix: bfloat16 [4096, 4096], P('kv', 'tp'), may hold values from -0.09375 to 0.09375
- result_sigmoid_matrix: bfloat16 [4096, 4096], P('kv', 'tp'), may hold values from -0.09375 to 0.09375
- storing_beta_matrix: bfloat16 [4096, 32], P('kv', 'tp'), may hold values from -0.09375 to 0.09375
- forgetting_matrix: bfloat16 [4096, 32], P('kv', 'tp'), may hold values from -0.09375 to 0.09375
- channel_forgetting_exponent: float32 [32], P('tp'), may hold values from -1 to 2
- forgetting_offset: float32 [32], P('tp'), may hold values from -3 to 0.5
- extra_forgetting: float32 [64, 32], P(('dp', 'kv'), 'tp'), may hold values from -0.7 to 0
- memory_matrices: float32 [64, 32, 128, 128], P(('dp', 'kv'), 'tp'), may hold values from -3 to 3
- channel_result_scaling: float32 [128], replicated, may hold values from 0.1 to 1.9
- mixer_exit_matrix: bfloat16 [4096, 4096], P('tp', 'kv'), may hold values from -0.09375 to 0.09375
- neuron_scaling_vector: float32 [4096], P(('kv', 'tp')), may hold values from 0.1 to 1.9
- widening_matrix: bfloat16 [4096, 16384], P(None, ('kv', 'tp')), may hold values from -0.09375 to 0.09375
- shrinking_matrix: bfloat16 [16384, 4096], P(('kv', 'tp')), may hold values from -0.0625 to 0.0625
Outputs:
- mixed: bfloat16 [64, 4096], P('dp', ('kv', 'tp'))
- new_state: float32 [64, 32, 128, 128], P(('dp', 'kv'), 'tp')
All inputs are finite; a program needn't handle non-finite values.
Results may differ from a plain program's by a relative error of at most 0.018.
Values may be sent and summed in bfloat16 or wider, within the bound.
A program may use at most 128 MiB of HBM per device.

v0:
```python
import jax
import jax.numpy as jnp
from jax import lax
from jax.sharding import PartitionSpec as P

D = 4096
KHEADS = 16
CONTENT_SLOTS = 32
HEAD = 128


epsilon = 1e-06


def unit_norm(values):
    return values * lax.rsqrt(jnp.sum(values * values, axis=-1, keepdims=True) + epsilon)


def rounded_product(left, right):
    return jnp.dot(left, right, preferred_element_type=jnp.float32).astype(jnp.bfloat16)


def on_device(
    incoming_vectors,
    mixer_scaling_vector,
    probe_matrix,
    address_matrix,
    content_matrix,
    result_sigmoid_matrix,
    storing_beta_matrix,
    forgetting_matrix,
    channel_forgetting_exponent,
    forgetting_offset,
    extra_forgetting,
    memory_matrices,
    channel_result_scaling,
    mixer_exit_matrix,
    neuron_scaling_vector,
    widening_matrix,
    shrinking_matrix,
):
    token_f = incoming_vectors.astype(jnp.float32)
    scaled = (token_f * mixer_scaling_vector).astype(jnp.bfloat16)
    part_square = jnp.sum(token_f * token_f, axis=1, keepdims=True)
    row_block, square_pair = (
        lax.all_gather(scaled, "tp", axis=1, tiled=True),
        lax.all_gather(part_square.astype(jnp.bfloat16), "tp", axis=1, tiled=True).astype(
            part_square.dtype
        ),
    )
    square = lax.psum(jnp.sum(square_pair, axis=1), "kv")
    inv_all = lax.rsqrt(square / D + epsilon)
    query_part = rounded_product(row_block, probe_matrix)
    key_part = rounded_product(row_block, address_matrix)
    value_part = rounded_product(row_block, content_matrix)
    gate_part = rounded_product(row_block, result_sigmoid_matrix)
    beta_part = rounded_product(row_block, storing_beta_matrix)
    decay_part = rounded_product(row_block, forgetting_matrix)
    query_sum, key_sum, value_sum, gate_sum, beta_sum, decay_total = (
        lax.psum_scatter(query_part, "kv", scatter_dimension=0, tiled=True).astype(jnp.float32),
        lax.psum_scatter(key_part, "kv", scatter_dimension=0, tiled=True).astype(jnp.float32),
        lax.psum_scatter(value_part, "kv", scatter_dimension=0, tiled=True).astype(jnp.float32),
        lax.psum_scatter(gate_part, "kv", scatter_dimension=0, tiled=True).astype(jnp.float32),
        lax.psum_scatter(beta_part, "kv", scatter_dimension=0, tiled=True).astype(jnp.float32),
        lax.psum_scatter(decay_part, "kv", scatter_dimension=0, tiled=True).astype(jnp.float32),
    )
    own_rows = query_sum.shape[0]
    inverse_root_mean = lax.dynamic_slice_in_dim(
        inv_all, lax.axis_index("kv") * own_rows, own_rows, 0
    )[:, None]
    repeat = CONTENT_SLOTS // KHEADS
    query = unit_norm((query_sum * inverse_root_mean).reshape(own_rows, -1, HEAD)) * HEAD ** (-0.5)
    key_n = unit_norm((key_sum * inverse_root_mean).reshape(own_rows, -1, HEAD))
    query = jnp.repeat(query, repeat, axis=1)
    key_n = jnp.repeat(key_n, repeat, axis=1)
    value = (value_sum * inverse_root_mean).reshape(own_rows, -1, HEAD)
    gate_raw = (gate_sum * inverse_root_mean).reshape(own_rows, -1, HEAD)
    beta = jax.nn.sigmoid(beta_sum * inverse_root_mean)
    forgetting_exponent = (
        -jnp.exp(channel_forgetting_exponent)
        * jax.nn.softplus(decay_total * inverse_root_mean + forgetting_offset)
        + extra_forgetting
    )
    decayed = jnp.exp(forgetting_exponent)[:, :, None, None] * memory_matrices
    predicted = jnp.einsum("shde,shd->she", decayed, key_n, precision=lax.Precision.HIGHEST)
    new_state = (
        decayed + beta[:, :, None, None] * key_n[:, :, :, None] * (value - predicted)[:, :, None, :]
    )
    head_out = jnp.einsum("shde,shd->she", new_state, query, precision=lax.Precision.HIGHEST)
    normed = head_out * lax.rsqrt(jnp.mean(head_out * head_out, axis=-1, keepdims=True) + epsilon)
    gated = (
        (normed * channel_result_scaling * jax.nn.silu(gate_raw))
        .astype(jnp.bfloat16)
        .reshape(own_rows, -1)
    )
    attn_part = rounded_product(lax.all_gather(gated, "kv", axis=0, tiled=True), mixer_exit_matrix)
    attn = lax.psum_scatter(attn_part, "tp", scatter_dimension=1, tiled=True).astype(jnp.float32)
    resid = (token_f + attn).astype(jnp.bfloat16)
    resid_f = resid.astype(jnp.float32)
    scaled2 = (resid_f * neuron_scaling_vector).astype(jnp.bfloat16)
    part_square2 = jnp.sum(resid_f * resid_f, axis=1, keepdims=True)
    full_hidden, square_hidden = (
        lax.all_gather(scaled2, ("kv", "tp"), axis=1, tiled=True),
        lax.all_gather(part_square2.astype(jnp.bfloat16), ("kv", "tp"), axis=1, tiled=True).astype(
            part_square2.dtype
        ),
    )
    inv_rms2 = lax.rsqrt(jnp.sum(square_hidden, axis=1, keepdims=True) / D + epsilon)
    up_raw = jax.nn.relu(
        jnp.dot(full_hidden, widening_matrix, preferred_element_type=jnp.float32) * inv_rms2
    )
    hidden = (up_raw * up_raw).astype(jnp.bfloat16)
    down_part = rounded_product(hidden, shrinking_matrix)
    down_sum = lax.psum_scatter(down_part, ("kv", "tp"), scatter_dimension=1, tiled=True).astype(
        jnp.float32
    )
    mixed = (resid_f + down_sum).astype(jnp.bfloat16)
    return (mixed, new_state)


def solution(mesh):
    return jax.shard_map(
        on_device,
        mesh=mesh,
        in_specs=(
            P("dp", ("kv", "tp")),
            P(("kv", "tp")),
            P("kv", "tp"),
            P("kv", "tp"),
            P("kv", "tp"),
            P("kv", "tp"),
            P("kv", "tp"),
            P("kv", "tp"),
            P("tp"),
            P("tp"),
            P(("dp", "kv"), "tp"),
            P(("dp", "kv"), "tp", None, None),
            P(),
            P("tp", "kv"),
            P(("kv", "tp")),
            P(None, ("kv", "tp")),
            P(("kv", "tp"), None),
        ),
        out_specs=(P("dp", ("kv", "tp")), P(("dp", "kv"), "tp", None, None)),
        check_vma=False,
    )
```

profile of v0, /device:TPU:0, one launch (start us, length us, event | category | flops | bytes accessed | tf_op | source)
XLA Modules:
  0.0 202.9 jit_solution(17667029198575852193)
XLA Ops:
  7.2 0.0 copy-start
  7.2 0.0 all-reduce.11.cloned.1.call-start
  7.2 1.0 fusion.9
  8.2 2.0 all_gather.15
  10.2 1.5 convolution_convert_fusion.6
  11.6 1.5 convolution_convert_fusion.7
  13.1 1.0 convolution_convert_fusion.4
  14.1 2.6 %convolution_convert_fusion.5 = bf16[16,1024]{1,0:T(8,128)(2,1)} fusion(bf16[16,1024]{1,0:T(8,128)(2,1)S(1)} %all_gather.15, bf16[1024,1024]{1,0:T(8,128)(2,1)} %param.20), kind=kOutput, calls=%fused_computation.13 | convolution fusion | flops 33570816 | bytes 2162688 | tf_op jit(solution)/shard_map/dot_general | solution.py:20
  16.7 0.0 all-reduce.11.cloned.1.call-update
  16.7 0.0 copy-start.10
  16.8 0.0 all-reduce.13.cloned.1.call-start
  16.8 0.0 copy-start.2
  16.8 3.6 %convolution_convert_fusion.1 = bf16[16,2048]{1,0:T(8,128)(2,1)} fusion(bf16[16,1024]{1,0:T(8,128)(2,1)S(1)} %all_gather.15, bf16[1024,2048]{1,0:T(8,128)(2,1)} %param.22), kind=kOutput, calls=%fused_computation.7 | convolution fusion | flops 67141632 | bytes 4292608 | tf_op jit(solution)/shard_map/dot_general | solution.py:20
  20.5 1.3 convolution_convert_fusion.2
  21.8 0.0 all-reduce.13.cloned.1.call-update
  21.8 0.0 reduce-scatter.3.cloned.1.call-start
  21.9 1.8 all-gather
  23.7 13.3 %psum.7 = f32[16]{0:T(128)S(1)} all-reduce(f32[16]{0:T(128)S(1)} %convert_reduce_fusion.1), channel_id=1, replica_groups=mesh['dp'=4,'kv'=4,'tp'=2] {'kv'}, use_global_device_ids=true, to_apply=%region_3.0 | all-reduce | flops 16 | bytes 128 | tf_op jit(solution)/shard_map/psum | solution.py:51
  37.0 0.6 dynamic-slice
  38.3 0.1 dynamic_slice.3
  38.4 15.7 %all-reduce.11.cloned.1.call-done = (bf16[16,1024]{1,0:T(8,128)(2,1)}, bf16[16,16]{1,0:T(8,128)(2,1)}, bf16[16,16]{1,0:T(8,128)(2,1)}, bf16[16,1024]{1,0:T(8,128)(2,1)}) async-done(((bf16[16,1024]{1,0:T(8,128)(2,1)}, bf16[16,16]{1,0:T(8,128)(2,1)}, bf16[16,16]{1,0:T(8,128)(2,1)}, bf16[16,1024]{1,0:T(8,128)(2,1)}), (bf16[16,1024]{1,0:T(8,128)(2,1)}, bf16[16,16]{1,0:T(8,128)(2,1)}, bf16[16,16]{1,0:T(8,128)(2,1)}, ...) | async-done | bytes 66576
  54.0 0.8 multiply_bitcast_fusion.2
  54.9 0.1 fusion.21
  55.0 0.1 fusion.19
  55.1 0.8 add_divide_fusion
  55.9 0.1 broadcast_multiply_fusion
  56.0 5.6 %fusion = f32[4,16,1,128]{3,2,1,0:T(1,128)S(1)} fusion(f32[4,16,128,1]{2,3,1,0:T(1,128)S(1)} %bitcast.79, f32[4,16,128,128]{3,2,1,0:T(8,128)} %param.28, f32[4,16]{1,0:T(4,128)S(1)} %get-tuple-element.15), kind=kOutput, calls=%fused_computation.2 | convolution fusion | flops 13631488 | bytes 4260096 | tf_op jit(solution)/shard_map/shde,shd->she/dot_general | solution.py:85
  61.6 0.1 fusion.20
  61.6 30.1 %all-reduce.13.cloned.1.call-done = (bf16[16,2048]{1,0:T(8,128)(2,1)}, bf16[16,2048]{1,0:T(8,128)(2,1)}) async-done(((bf16[16,2048]{1,0:T(8,128)(2,1)}, bf16[16,2048]{1,0:T(8,128)(2,1)}), (bf16[16,2048]{1,0:T(8,128)(2,1)}, bf16[16,2048]{1,0:T(8,128)(2,1)})) %all-reduce.13.cloned.1.call-update) | async-done | bytes 131088
  91.7 0.9 multiply_bitcast_fusion.1
  92.6 3.1 %multiply_add_fusion = f32[4,16,128,128]{3,2,1,0:T(8,128)S(1)} fusion(f32[4,16,128,128]{3,2,1,0:T(8,128)} %param.28, f32[4,16,128]{2,1,0:T(8,128)S(1)} %bitcast_subtract_fusion, f32[4,16,128]{2,1,0:T(8,128)S(1)} %broadcast_multiply_fusion, f32[4,16]{1,0:T(4,128)S(1)} %get-tuple-element.15), kind=kLoop, calls=%fused_computation.1 | loop fusion | flops 3145728 | bytes 8454400 | tf_op jit(solution)/shard_map/add | solution.py:87
  95.6 0.0 copy-start.1
  95.7 2.0 copy-done.1
  97.7 3.6 %fusion.26 = f32[4,16,1,128]{3,2,1,0:T(1,128)S(1)} fusion(f32[4,16,128,128]{3,2,1,0:T(8,128)S(1)} %multiply_add_fusion, f32[4,16,128,1]{2,3,1,0:T(1,128)S(1)} %bitcast.83), kind=kOutput, calls=%fused_computation.69 | convolution fusion | flops 12582912 | bytes 4259840 | tf_op jit(solution)/shard_map/shde,shd->she/dot_general | solution.py:89
  101.3 0.1 multiply_reduce_fusion
  101.4 0.1 fusion.18
  101.5 13.1 %all-gather.1 = bf16[4,4,2048]{2,1,0:T(4,128)(2,1)S(1)} all-gather(bf16[1,4,2048]{2,1,0:T(4,128)(2,1)S(1)} %reshape.95), channel_id=1, replica_groups=mesh['dp'=4,'kv'=4,'tp'=2] {'kv'}, dimensions={0}, use_global_device_ids=true | all-gather | bytes 81920 | tf_op jit(solution)/shard_map/all_gather | solution.py:96
  114.7 3.4 %convolution_convert_fusion.3 = bf16[16,1024]{1,0:T(8,128)(2,1)} fusion(bf16[16,2048]{1,0:T(8,128)(2,1)S(1)} %reshape.96, bf16[2048,1024]{1,0:T(8,128)(2,1)} %param.30), kind=kOutput, calls=%fused_computation.11 | convolution fusion | flops 67125248 | bytes 4292608 | tf_op jit(solution)/shard_map/dot_general | solution.py:20
  118.1 0.0 reduce-scatter.3.cloned.1.call-update
  118.2 0.0 reduce-scatter.5.cloned.1.call-start
  118.2 7.4 %reduce-scatter.3.cloned.1.call-done = bf16[16,512]{1,0:T(8,128)(2,1)} async-done(((bf16[16,1024]{1,0:T(8,128)(2,1)}), bf16[16,512]{1,0:T(8,128)(2,1)}) %reduce-scatter.3.cloned.1.call-update) | async-done | bytes 16400 | tf_op jit(solution)/shard_map/reduce_scatter | solution.py:97
  125.6 0.8 fusion.12
  126.5 11.9 %all-gather.2 = bf16[8,1,16]{2,1,0:T(2,128)(2,1)S(1)} all-gather(bf16[1,1,16]{2,1,0:T(2,128)(2,1)S(1)} %bitcast.84), channel_id=1, replica_groups=mesh['dp'=4,'kv'=4,'tp'=2] {'kv','tp'}, dimensions={0}, use_global_device_ids=true | all-gather | bytes 288 | tf_op jit(solution)/shard_map/all_gather | solution.py:104
  138.4 14.2 %all_gather.18 = bf16[16,4096]{1,0:T(8,128)(2,1)S(1)} all-gather(bf16[16,512]{1,0:T(8,128)(2,1)S(1)} %get-tuple-element.9), channel_id=1, replica_groups=mesh['dp'=4,'kv'=4,'tp'=2] {'kv','tp'}, dimensions={1}, use_global_device_ids=true | all-gather | bytes 147456 | tf_op jit(solution)/shard_map/all_gather | solution.py:103
  152.6 13.5 %convolution_convert_fusion = bf16[16,4096]{1,0:T(8,128)(2,1)} fusion(bf16[2048,4096]{1,0:T(8,128)(2,1)} %param.33, bf16[16,4096]{1,0:T(8,128)(2,1)S(1)} %all_gather.18, bf16[4096,2048]{1,0:T(8,128)(2,1)} %param.32, f32[16]{0:T(128)S(1)} %add_rsqrt_fusion.3), kind=kOutput, calls=%fused_computation | convolution fusion | flops 537067520 | bytes 33816640 | tf_op jit(solution)/shard_map/dot_general | solution.py:20
  166.1 0.0 reduce-scatter.5.cloned.1.call-update
  166.1 28.9 %reduce-scatter.5.cloned.1.call-done = bf16[16,512]{1,0:T(8,128)(2,1)} async-done(((bf16[16,4096]{1,0:T(8,128)(2,1)}), bf16[16,512]{1,0:T(8,128)(2,1)}) %reduce-scatter.5.cloned.1.call-update) | async-done | bytes 16400 | tf_op jit(solution)/shard_map/reduce_scatter | solution.py:114
  195.0 1.3 fusion.13
  (30 shorter events, 0.2 us)
Async XLA Ops:
  7.2 6.0 %copy-start = (bf16[1024,1024]{1,0:T(8,128)(2,1)S(1)}, bf16[1024,1024]{1,0:T(8,128)(2,1)}, u32[]{:S(2)}) copy-start(bf16[1024,1024]{1,0:T(8,128)(2,1)} %param.19) | copy-start | bytes 6291460
  7.2 46.9 %all-reduce.11.cloned.1.call-start = ((), (), s32[]{:S(2)}) async-start(), calls=%async_computation.4 | async-start | bytes 147456
  16.7 5.1 %copy-start.9 = (f32[16]{0:T(128)S(1)}, f32[16]{0:T(128)}, u32[]{:S(2)}) copy-start(f32[16]{0:T(128)} %param.25) | copy-start | bytes 196
  16.7 20.3 %copy-start.10 = (u32[32]{0:T(128)S(1)}, u32[32]{0:T(128)}, u32[]{:S(2)}) copy-start(u32[32]{0:T(128)} %constant.41) | copy-start | bytes 388
  16.7 38.3 %copy-start.5 = (f32[4,16]{1,0:T(4,128)S(1)}, f32[4,16]{1,0:T(4,128)}, u32[]{:S(2)}) copy-start(f32[4,16]{1,0:T(4,128)} %param.27) | copy-start | bytes 772
  16.8 38.3 %copy-start.8 = (f32[16]{0:T(128)S(1)}, f32[16]{0:T(128)}, u32[]{:S(2)}) copy-start(f32[16]{0:T(128)} %param.26) | copy-start | bytes 196
  16.8 74.9 %all-reduce.13.cloned.1.call-start = ((), (), s32[]{:S(2)}) async-start(), calls=%async_computation.5 | async-start | bytes 262144
  16.8 3.6 %copy-start.2 = (bf16[1024,2048]{1,0:T(8,128)(2,1)S(1)}, bf16[1024,2048]{1,0:T(8,128)(2,1)}, u32[]{:S(2)}) copy-start(bf16[1024,2048]{1,0:T(8,128)(2,1)} %param.21) | copy-start | bytes 12582916
  21.8 103.8 %reduce-scatter.3.cloned.1.call-start = ((), (), s32[]{:S(2)}) async-start(), calls=%async_computation.2 | async-start | bytes 49152 | tf_op jit(solution)/shard_map/reduce_scatter | solution.py:97
  95.6 2.0 copy-start.1
  95.7 5.8 %copy-start.7 = (f32[128]{0:T(128)S(1)}, f32[128]{0:T(128)}, u32[]{:S(2)}) copy-start(f32[128]{0:T(128)} %param.29) | copy-start | bytes 1540
  97.7 27.9 %copy-start.3 = (bf16[16,512]{1,0:T(8,128)(2,1)S(1)}, bf16[16,512]{1,0:T(8,128)(2,1)}, u32[]{:S(2)}) copy-start(bf16[16,512]{1,0:T(8,128)(2,1)} %param.17) | copy-start | bytes 49156
  97.7 27.9 %copy-start.6 = (f32[512]{0:T(512)S(1)}, f32[512]{0:T(512)}, u32[]{:S(2)}) copy-start(f32[512]{0:T(512)} %param.31) | copy-start | bytes 6148
  118.2 76.8 %reduce-scatter.5.cloned.1.call-start = ((), (), s32[]{:S(2)}) async-start(), calls=%async_computation.3 | async-start | bytes 147456 | tf_op jit(solution)/shard_map/reduce_scatter | solution.py:114
  152.6 42.4 %copy-start.4 = (bf16[16,512]{1,0:T(8,128)(2,1)S(1)}, bf16[16,512]{1,0:T(8,128)(2,1)}, u32[]{:S(2)}) copy-start(bf16[16,512]{1,0:T(8,128)(2,1)} %reduce-scatter.3.cloned.1.call-done) | copy-start | bytes 49156
Sparse Core Ops, SparseCore 0:
  16.8 37.1 all-reduce.10
  57.0 34.6 all-reduce.12
  118.3 7.2 reduce-scatter.2
  166.2 28.7 reduce-scatter.4
where the time goes:
time: 204 us; the launch traced here: 203 us
  waiting for transfers between devices  82.1 us (40%)
  blocking collectives  56.3 us (28%)
  matrix products  37.6 us (18%)
  between operations  14.6 us (7%)
  other arithmetic  9.24 us (5%)
  local copies, waits for them, and re-layouts  2.8 us (1%)
    unnamed x6, waiting for transfers between devices  45.8 us
    reduce_scatter x1, waiting for transfers between devices, on_device(): lax.psum_scatter(down_part, ('kv', 'tp'), scatter_dimension=1, tiled=True)  28.9 us
    dot_general x8, matrix products, rounded_product(): jnp.dot(left, right, preferred_element_type=jnp.float32)  28.4 us
    all_gather x1, blocking collectives, on_device(): lax.all_gather(scaled2, ('kv', 'tp'), axis=1, tiled=True)  14.2 us
    psum x1, blocking collectives, on_device(): square = lax.psum(jnp.sum(square_pair, axis=1), 'kv')  13.3 us
    all_gather x1, blocking collectives, on_device(): lax.all_gather(gated, 'kv', axis=0, tiled=True)  13.1 us
    all_gather x1, blocking collectives, on_device(): lax.all_gather(part_square2.astype(jnp.bfloat16), ('kv', 'tp'), axis=1, t...  11.9 us
    reduce_scatter x1, waiting for transfers between devices, on_device(): lax.psum_scatter(attn_part, 'tp', scatter_dimension=1, tiled=True)  7.4 us
  transfers between devices with their start and end apart: 4, of which 4 were waited for; matrix products, arithmetic and copies ran while one was open for 6% of the time, Pallas kernels for 0%

commit v1 on v0

v1 whole, which is shorter than its diff:
```python
import functools

import jax
import jax.numpy as jnp
from jax import lax
from jax.experimental import pallas as pl
from jax.experimental.pallas import tpu as pltpu
from jax.sharding import PartitionSpec as P

MESH = pl.DeviceIdType.MESH
EPS = 1e-06
F32 = jnp.float32
BF16 = jnp.bfloat16


def dot(left, right):
    return jnp.dot(left, right, preferred_element_type=F32)


def layer(
    KV, TP, D,
    x, g1, wq, wk, wv, wg, wb, wd, fexp, foff, extra, mem, crs, wo, g2, wu, ws,
    mixed, new_state,
    xb, g1b, g2b, vq, vk, vv, vg, vb, vd, vfexp, vfoff, vextra, st, vcrs, vo, vu, vs,
    qst, qrc, vst, vrc, gst, grc, sst, src, kq, ho, gall, ap, rb, up, hid, dst, drc, mo,
    lsem, usem, ssem, osem,
    bs, br, x_s, x_r, p_s, p_r, a_s, a_r, t_s, t_r, r_s, r_r, d_s, d_r,
):
    kv, tp = lax.axis_index("kv"), lax.axis_index("tp")
    N = KV * TP
    flat = kv * TP + tp
    R, C = x.shape
    own = R // KV
    K1 = TP * C
    heads = st.shape[1]
    HEAD = st.shape[2]
    khe = wq.shape[1] // HEAD
    rep = heads // khe
    QC, VC = wq.shape[1], wv.shape[1]

    def local(i, a, b):
        c = pltpu.make_async_copy(a, b, lsem.at[i])
        c.start()
        return c

    cx = local(0, x, xb.at[tp])
    cg1 = local(1, g1, g1b.at[tp])
    cg2 = local(2, g2, g2b.at[flat])
    cq = local(3, wq, vq)
    ck = local(4, wk, vk)
    cb = local(5, wb, vb)
    cd = local(6, wd, vd)
    cv = local(7, wv, vv)
    cg = local(8, wg, vg)
    smalls = [
        local(9, fexp, vfexp), local(10, foff, vfoff), local(11, extra, vextra),
        local(12, crs, vcrs),
    ]

    barrier = pltpu.get_barrier_semaphore()
    for s in range(1, N):
        other = lax.rem(flat + s, N)
        pl.semaphore_signal(
            barrier, inc=1, device_id={"kv": other // TP, "tp": lax.rem(other, TP)},
            device_id_type=MESH,
        )
    pl.semaphore_wait(barrier, N - 1)

    def remote(a, b, ss, rs, okv, otp):
        return pltpu.make_async_remote_copy(
            src_ref=a, dst_ref=b, send_sem=ss, recv_sem=rs,
            device_id={"kv": okv, "tp": otp}, device_id_type=MESH,
        )

    sends = []
    for s in range(1, TP):
        o = lax.rem(tp + s, TP)
        c = remote(x, xb.at[tp], x_s.at[0, o], x_r.at[0, tp], kv, o)
        c.start()
        sends.append(c)
        c = remote(g1, g1b.at[tp], x_s.at[1, o], x_r.at[1, tp], kv, o)
        c.start()
        sends.append(c)
    for s in range(1, N):
        o = lax.rem(flat + s, N)
        c = remote(g2, g2b.at[flat], bs.at[o], br.at[flat], o // TP, lax.rem(o, TP))
        c.start()
        sends.append(c)
    cst = local(13, mem, st)
    co = local(14, wo, vo)

    cx.wait()
    cg1.wait()
    for s in range(1, TP):
        o = lax.rem(tp + s, TP)
        remote(x, xb.at[o], x_s.at[0, o], x_r.at[0, o], kv, o).wait_recv()
        remote(g1, g1b.at[o], x_s.at[1, o], x_r.at[1, o], kv, o).wait_recv()
    xf = jnp.concatenate([xb[t] for t in range(TP)], axis=1).astype(F32)
    gf = jnp.concatenate([g1b[t] for t in range(TP)], axis=1)
    scaled = (xf * gf).astype(BF16)
    ssq = jnp.broadcast_to(jnp.sum(xf * xf, axis=1, keepdims=True), (R, 128))
    for p in range(KV):
        sst[p] = ssq[p * own:(p + 1) * own]

    def scatter(stage, rec, i):
        for s in range(1, KV):
            o = lax.rem(kv + s, KV)
            c = remote(stage.at[o], rec.at[kv], p_s.at[i, o], p_r.at[i, kv], o, tp)
            c.start()
            sends.append(c)
        rec[kv] = stage[kv]

    def arrive(stage, rec, i):
        for s in range(1, KV):
            o = lax.rem(kv + s, KV)
            remote(stage.at[o], rec.at[o], p_s.at[i, o], p_r.at[i, o], o, tp).wait_recv()
        total = rec[0].astype(F32)
        for p in range(1, KV):
            total = total + rec[p].astype(F32)
        return total

    scatter(sst, src, 0)

    def project(w, stage, base):
        cols = w.shape[1]
        step = min(cols, 1024)
        for c in range(cols // step):
            part = dot(scaled, w[:, c * step:(c + 1) * step])
            for p in range(KV):
                stage[p, :, base + c * step:base + (c + 1) * step] = part[
                    p * own:(p + 1) * own
                ].astype(BF16)

    cq.wait()
    project(vq, qst, 0)
    ck.wait()
    project(vk, qst, QC)
    ups = []
    for s in range(KV):
        o = lax.rem(kv + s, KV)
        rows = pl.ds(pl.multiple_of(o * K1, K1), K1)
        c = pltpu.make_async_copy(wu.at[rows], vu.at[rows], usem.at[s])
        c.start()
        ups.append(c)
    cb.wait()
    cd.wait()
    project(vb, qst, 2 * QC)
    project(vd, qst, 2 * QC + 128)
    scatter(qst, qrc, 1)
    cv.wait()
    project(vv, vst, 0)
    scatter(vst, vrc, 2)
    downs = []
    SR = ws.shape[0] // 4
    for s in range(4):
        rows = pl.ds(s * SR, SR)
        c = pltpu.make_async_copy(ws.at[rows], vs.at[rows], ssem.at[s])
        c.start()
        downs.append(c)
    cg.wait()
    project(vg, gst, 0)
    scatter(gst, grc, 3)

    for c in smalls:
        c.wait()
    inv = lax.rsqrt(arrive(sst, src, 0)[:, 0:1] * (1.0 / D) + EPS)
    qk = arrive(qst, qrc, 1) * inv
    beta = jax.nn.sigmoid(qk[:, 2 * QC:2 * QC + heads])
    z = qk[:, 2 * QC + 128:2 * QC + 128 + heads] + vfoff[...]
    soft = jnp.maximum(z, 0.0) + jnp.log1p(jnp.exp(-jnp.abs(z)))
    decay = jnp.exp(vextra[...] - jnp.exp(vfexp[...]) * soft)
    kqd = []
    half = khe * own
    for h in range(khe):
        q_h = qk[:, h * HEAD:(h + 1) * HEAD]
        k_h = qk[:, QC + h * HEAD:QC + (h + 1) * HEAD]
        q_h = q_h * (
            lax.rsqrt(jnp.sum(q_h * q_h, axis=1, keepdims=True) + EPS) * HEAD ** (-0.5)
        )
        k_h = k_h * lax.rsqrt(jnp.sum(k_h * k_h, axis=1, keepdims=True) + EPS)
        kqd.append(jnp.sum(q_h * k_h, axis=1, keepdims=True))
        kq[h * own:(h + 1) * own, :] = k_h
        kq[half + h * own:half + (h + 1) * own, :] = q_h
    kqt = jnp.transpose(kq[...])
    value = arrive(vst, vrc, 2) * inv
    cst.wait()
    outs = []
    for hk in range(khe):
        for s in range(own):
            i = hk * own + s
            kcol = kqt[:, i:i + 1]
            qcol = kqt[:, half + i:half + i + 1]
            kd = kqd[hk][s:s + 1]
            for r in range(rep):
                h = hk * rep + r
                S = st[s, h]
                a = decay[s:s + 1, h:h + 1]
                pk = jnp.sum(S * kcol, axis=0, keepdims=True)
                pq = jnp.sum(S * qcol, axis=0, keepdims=True)
                u = beta[s:s + 1, h:h + 1] * (
                    value[s:s + 1, h * HEAD:(h + 1) * HEAD] - a * pk
                )
                ho[s:s + 1, h * HEAD:(h + 1) * HEAD] = a * pq + kd * u
                st[s, h] = a * S + kcol * u
        hs = pl.ds(hk * rep, rep)
        c = pltpu.make_async_copy(st.at[:, hs], new_state.at[:, hs], osem.at[hk])
        c.start()
        outs.append(c)

    gate = arrive(gst, grc, 3) * inv
    for h in range(heads):
        cols = slice(h * HEAD, (h + 1) * HEAD)
        o_h = ho[:, cols]
        v = gate[:, cols]
        n_h = o_h * lax.rsqrt(jnp.mean(o_h * o_h, axis=1, keepdims=True) + EPS)
        gall[kv, :, cols] = (n_h * vcrs[...] * (v / (1.0 + jnp.exp(-v)))).astype(BF16)
    for s in range(1, KV):
        o = lax.rem(kv + s, KV)
        c = remote(gall.at[kv], gall.at[kv], a_s.at[o], a_r.at[kv], o, tp)
        c.start()
        sends.append(c)
    co.wait()
    for s in range(1, KV):
        o = lax.rem(kv + s, KV)
        remote(gall.at[o], gall.at[o], a_s.at[o], a_r.at[o], o, tp).wait_recv()
    gated = jnp.concatenate([gall[p].astype(F32) for p in range(KV)], axis=0).astype(BF16)
    ap[tp] = dot(gated, vo[...]).astype(BF16)
    for s in range(1, TP):
        o = lax.rem(tp + s, TP)
        c = remote(ap.at[tp], ap.at[tp], t_s.at[o], t_r.at[tp], kv, o)
        c.start()
        sends.append(c)
    for s in range(1, TP):
        o = lax.rem(tp + s, TP)
        remote(ap.at[o], ap.at[o], t_s.at[o], t_r.at[o], kv, o).wait_recv()
    attn = ap[0].astype(F32)
    for t in range(1, TP):
        attn = attn + ap[t].astype(F32)
    xf = jnp.concatenate([xb[t] for t in range(TP)], axis=1).astype(F32)
    rb[kv] = (xf + attn).astype(BF16)
    for s in range(1, KV):
        o = lax.rem(kv + s, KV)
        c = remote(rb.at[kv], rb.at[kv], r_s.at[o], r_r.at[kv], o, tp)
        c.start()
        sends.append(c)

    cg2.wait()
    for s in range(1, N):
        o = lax.rem(flat + s, N)
        remote(g2, g2b.at[o], bs.at[o], br.at[o], o // TP, lax.rem(o, TP)).wait_recv()
    ssq2 = jnp.zeros((R, 1), F32)
    UC = wu.shape[1]
    ustep = min(UC, 1024)
    for s in range(KV):
        o = lax.rem(kv + s, KV)
        if s:
            remote(rb.at[o], rb.at[o], r_s.at[o], r_r.at[o], o, tp).wait_recv()
        ups[s].wait()
        res = rb[o].astype(F32)
        ssq2 = ssq2 + jnp.sum(res * res, axis=1, keepdims=True)
        gain = jnp.concatenate([g2b[o * TP + t] for t in range(TP)], axis=1)
        sc = (res * gain).astype(BF16)
        rows = pl.ds(pl.multiple_of(o * K1, K1), K1)
        for c in range(UC // ustep):
            cols = slice(c * ustep, (c + 1) * ustep)
            part = dot(sc, vu[rows, cols])
            if s:
                part = part + up[:, cols]
            up[:, cols] = part
    inv2 = lax.rsqrt(ssq2 * (1.0 / D) + EPS)
    hv = jnp.maximum(up[...] * inv2, 0.0)
    hid[...] = (hv * hv).astype(BF16)
    for c in downs:
        c.wait()

    def down(t, carry):
        i, j = t // TP, lax.rem(t, TP)
        step = (i + 1) // 2
        okv = lax.rem(
            kv + KV // 2 + jnp.where(lax.rem(i, 2) == 0, step, -step) + KV, KV
        )
        otp = lax.rem(tp + TP - 1 - j, TP)
        o = okv * TP + otp
        part = dot(hid[...], vs[:, pl.ds(pl.multiple_of(o * C, C), C)])
        dst[o] = part.astype(BF16)

        @pl.when(t < N - 1)
        def _():
            remote(dst.at[o], drc.at[flat], d_s.at[o], d_r.at[flat], okv, otp).start()

        return carry

    lax.fori_loop(0, N, down, 0)
    total = rb[kv, :, pl.ds(pl.multiple_of(tp * C, C), C)].astype(F32) + dst[flat].astype(F32)
    for s in range(1, N):
        o = lax.rem(flat + s, N)
        remote(dst.at[o], drc.at[o], d_s.at[o], d_r.at[o], o // TP, lax.rem(o, TP)).wait_recv()
        total = total + drc[o].astype(F32)
    mo[...] = total.astype(BF16)
    last = pltpu.make_async_copy(mo, mixed, osem.at[khe])
    last.start()
    for c in sends:
        c.wait_send()
    for s in range(1, N):
        o = lax.rem(flat + s, N)
        remote(dst.at[o], drc.at[o], d_s.at[o], d_r.at[o], o // TP, lax.rem(o, TP)).wait_send()
    for c in outs:
        c.wait()
    last.wait()


def solution(mesh):
    KV, TP = mesh.shape["kv"], mesh.shape["tp"]

    def on_device(x, g1, wq, wk, wv, wg, wb, wd, fexp, foff, extra, mem, crs, wo, g2, wu, ws):
        R, C = x.shape
        N = KV * TP
        D = C * N
        own, heads, HEAD, _ = mem.shape
        QC, VC = wq.shape[1], wv.shape[1]
        khe = QC // HEAD
        K1 = C * TP
        V = pltpu.VMEM
        S = pltpu.SemaphoreType.DMA
        args = (
            x, g1[None], wq, wk, wv, wg, wb, wd, fexp[None], foff[None], extra, mem,
            crs[None], wo, g2[None], wu, ws,
        )
        kqr = -(-2 * khe * own // 128) * 128
        scratch = [
            V((TP, R, C), BF16), V((TP, 1, C), F32), V((N, 1, C), F32),
            V(wq.shape, BF16), V(wk.shape, BF16), V(wv.shape, BF16), V(wg.shape, BF16),
            V(wb.shape, BF16), V(wd.shape, BF16),
            V((1, heads), F32), V((1, heads), F32), V(extra.shape, F32),
            V(mem.shape, F32), V((1, HEAD), F32),
            V(wo.shape, BF16), V(wu.shape, BF16), V(ws.shape, BF16),
            V((KV, own, 2 * QC + 256), BF16), V((KV, own, 2 * QC + 256), BF16),
            V((KV, own, VC), BF16), V((KV, own, VC), BF16),
            V((KV, own, VC), BF16), V((KV, own, VC), BF16),
            V((KV, own, 128), F32), V((KV, own, 128), F32),
            V((kqr, HEAD), F32), V((own, VC), F32),
            V((KV, own, VC), BF16), V((TP, R, K1), BF16), V((KV, R, K1), BF16),
            V((R, wu.shape[1]), F32), V((R, wu.shape[1]), BF16),
            V((N, R, C), BF16), V((N, R, C), BF16), V((R, C), BF16),
            S((15,)), S((KV,)), S((4,)), S((khe + 1,)),
            S((N,)), S((N,)), S((2, TP)), S((2, TP)), S((4, KV)), S((4, KV)),
            S((KV,)), S((KV,)), S((TP,)), S((TP,)), S((KV,)), S((KV,)), S((N,)), S((N,)),
        ]
        any_spec = pl.BlockSpec(memory_space=pl.ANY)
        return pl.pallas_call(
            functools.partial(layer, KV, TP, D),
            out_shape=(
                jax.ShapeDtypeStruct((R, C), BF16),
                jax.ShapeDtypeStruct(mem.shape, F32),
            ),
            in_specs=[any_spec] * len(args),
            out_specs=(any_spec, any_spec),
            scratch_shapes=scratch,
            compiler_params=pltpu.CompilerParams(
                collective_id=0, has_side_effects=True, vmem_limit_bytes=67043328
            ),
            name="layer",
        )(*args)

    return jax.shard_map(
        on_device,
        mesh=mesh,
        in_specs=(
            P("dp", ("kv", "tp")),
            P(("kv", "tp")),
            P("kv", "tp"),
            P("kv", "tp"),
            P("kv", "tp"),
            P("kv", "tp"),
            P("kv", "tp"),
            P("kv", "tp"),
            P("tp"),
            P("tp"),
            P(("dp", "kv"), "tp"),
            P(("dp", "kv"), "tp", None, None),
            P(),
            P("tp", "kv"),
            P(("kv", "tp")),
            P(None, ("kv", "tp")),
            P(("kv", "tp"), None),
        ),
        out_specs=(P("dp", ("kv", "tp")), P(("dp", "kv"), "tp", None, None)),
        check_vma=False,
    )
```

time: 204 us -> 43.2 us (0.21)
  waiting for transfers between devices: 82.1 us -> 0 us
  blocking collectives: 56.3 us -> 0 us
  matrix products: 37.6 us -> 0 us
  Pallas kernels: 0 us -> 33 us
  between operations: 14.6 us -> 0.64 us
  other arithmetic: 9.24 us -> 0 us
  local copies, waits for them, and re-layouts: 2.8 us -> 9.21 us
    unnamed x6 -> x0, waiting for transfers between devices: 45.8 us -> none
    all_gather x5 -> x0, blocking collectives: 43 us -> none  [the longest x1 14.2 us: on_device(): lax.all_gather(scaled2, ('kv', 'tp'), axis=1, tiled=True)]
    dot_general x10 -> x0, matrix products: 37.6 us -> none  [the longest x8 28.4 us: rounded_product(): jnp.dot(left, right, preferred_element_type=jnp.float32)]
    reduce_scatter x2 -> x0, waiting for transfers between devices: 36.3 us -> none  [the longest x1 28.9 us: on_device(): lax.psum_scatter(down_part, ('kv', 'tp'), scatter_dimension=1, tiled=True)]
    pallas_call x0 -> x1, Pallas kernels: none -> 33 us  [on_device(): pl.pallas_call(functools.partial(layer, KV, TP, D), out_shape=(jax.ShapeD...]
    psum x1 -> x0, blocking collectives: 13.3 us -> none  [on_device(): square = lax.psum(jnp.sum(square_pair, axis=1), 'kv')]
    unnamed x25 -> x4, local copies, waits for them, and re-layouts: 2.69 us -> 9.21 us
    add x1 -> x0, other arithmetic: 3.07 us -> none  [on_device(): decayed + beta[:, :, None, None] * key_n[:, :, :, None] * (value - predic...]
  transfers between devices with their start and end apart: 4 -> 0, of which waited for: 4 -> 0; matrix products, arithmetic and copies ran while one was open for 6% -> 0% of each run, Pallas kernels for 0% -> 0%
where the time goes in v1:
time: 43.2 us; the launch traced here: 42.9 us
  Pallas kernels  33 us (76%)
  local copies, waits for them, and re-layouts  9.21 us (21%)
  between operations  0.64 us (1%)
    pallas_call x1, Pallas kernels, on_device(): pl.pallas_call(functools.partial(layer, KV, TP, D), out_shape=(jax.ShapeD...  33 us
    unnamed x4, local copies, waits for them, and re-layouts  9.21 us

profile of v1, /device:TPU:0, one launch (start us, length us, event | category | flops | bytes accessed | tf_op | source)
XLA Modules:
  0.0 42.9 jit_solution(12748924918713045261)
XLA Ops:
  0.6 1.6 %copy.19.wb = bf16[1024,16]{1,0:T(8,128)(2,1)} copy(bf16[1024,16]{0,1:T(8,128)(2,1)} %param.23) | data formatting | bytes 65536 | tf_op args[6]
  2.2 1.6 %copy.20.wd = bf16[1024,16]{1,0:T(8,128)(2,1)} copy(bf16[1024,16]{0,1:T(8,128)(2,1)} %param.24) | data formatting | bytes 65536 | tf_op args[7]
  3.8 33.0 %layer.1 = (bf16[16,512]{1,0:T(8,128)(2,1)}, f32[4,16,128,128]{3,2,1,0:T(8,128)}) custom-call(bf16[16,512]{1,0:T(8,128)(2,1)} %x.1, f32[1,512]{1,0:T(1,128)} %bitcast.5, bf16[1024,1024]{1,0:T(8,128)(2,1)} %wq.1, bf16[1024,1024]{1,0:T(8,128)(2,1)} %wk.1, bf16[1024,2048]{1,0:T(8,128)(2,1)} %wv.1, bf16[1024,2048]{1,0:T(8,128)(2,1)} %wg.1, ...), custom_call_target="tpu_custom_call" | custom-call | tf_op jit(solution)/shard_map/layer/pallas_call | solution.py:350
  36.8 1.3 %copy.23 = bf16[16,512]{1,0:T(8,128)(2,1)} copy(bf16[16,512]{1,0:T(8,128)(2,1)} %get-tuple-element.4) | data formatting | bytes 32768
  38.2 4.7 %copy.24 = f32[4,16,128,128]{3,2,1,0:T(8,128)} copy(f32[4,16,128,128]{3,2,1,0:T(8,128)} %get-tuple-element.5) | data formatting | bytes 8388608

commit v2 on v1

--- a/solution.py
+++ b/solution.py
@@ -11,6 +11,7 @@
 EPS = 1e-06
 F32 = jnp.float32
 BF16 = jnp.bfloat16
+VMEM_LIMIT = 58 << 20
 
 
 def dot(left, right):
@@ -20,10 +21,10 @@
 def layer(
     KV, TP, D,
     x, g1, wq, wk, wv, wg, wb, wd, fexp, foff, extra, mem, crs, wo, g2, wu, ws,
-    mixed, new_state,
-    xb, g1b, g2b, vq, vk, vv, vg, vb, vd, vfexp, vfoff, vextra, st, vcrs, vo, vu, vs,
-    qst, qrc, vst, vrc, gst, grc, sst, src, kq, ho, gall, ap, rb, up, hid, dst, drc, mo,
-    lsem, usem, ssem, osem,
+    mo, st,
+    xb, g1b, g2b, vq, vk, vv, vg, vb, vd, vfexp, vfoff, vextra, vcrs, vo, vu, vs,
+    qst, qrc, vst, vrc, gst, grc, sst, src, kq, ho, gall, ap, rb, up, hid, dst, drc, pacc,
+    lsem, usem, ssem,
     bs, br, x_s, x_r, p_s, p_r, a_s, a_r, t_s, t_r, r_s, r_r, d_s, d_r,
 ):
     kv, tp = lax.axis_index("kv"), lax.axis_index("tp")
@@ -86,11 +87,25 @@
         c = remote(g2, g2b.at[flat], bs.at[o], br.at[flat], o // TP, lax.rem(o, TP))
         c.start()
         sends.append(c)
+    cx.wait()
+    cg1.wait()
+    mine = (xb[tp].astype(F32) * g1b[tp]).astype(BF16)
+
+    def first(w, base):
+        cols = w.shape[1]
+        step = min(cols, 1024)
+        rows = pl.ds(pl.multiple_of(tp * C, C), C)
+        for c in range(cols // step):
+            pacc[:, base + c * step:base + (c + 1) * step] = dot(
+                mine, w[rows, c * step:(c + 1) * step]
+            )
+
+    cq.wait()
+    first(vq, 0)
+    ck.wait()
+    first(vk, QC)
     cst = local(13, mem, st)
     co = local(14, wo, vo)
-
-    cx.wait()
-    cg1.wait()
     for s in range(1, TP):
         o = lax.rem(tp + s, TP)
         remote(x, xb.at[o], x_s.at[0, o], x_r.at[0, o], kv, o).wait_recv()
@@ -121,6 +136,28 @@
 
     scatter(sst, src, 0)
 
+    def rest(w, stage, base):
+        cols = w.shape[1]
+        step = min(cols, 1024)
+        for c in range(cols // step):
+            part = pacc[:, base + c * step:base + (c + 1) * step]
+            for s in range(1, TP):
+                o = lax.rem(tp + s, TP)
+                x_o = (xb[o].astype(F32) * g1b[o]).astype(BF16)
+                rows = pl.ds(pl.multiple_of(o * C, C), C)
+                part = part + dot(x_o, w[rows, c * step:(c + 1) * step])
+            for p in range(KV):
+                stage[p, :, base + c * step:base + (c + 1) * step] = part[
+                    p * own:(p + 1) * own
+                ].astype(BF16)
+
+    def small(w, stage, base):
+        part = lax.dot_general(
+            scaled, w[...], (((1,), (1,)), ((), ())), preferred_element_type=F32
+        )
+        for p in range(KV):
+            stage[p, :, base:base + heads] = part[p * own:(p + 1) * own].astype(BF16)
+
     def project(w, stage, base):
         cols = w.shape[1]
         step = min(cols, 1024)
@@ -131,10 +168,14 @@
                     p * own:(p + 1) * own
                 ].astype(BF16)
 
-    cq.wait()
-    project(vq, qst, 0)
-    ck.wait()
-    project(vk, qst, QC)
+    rest(vq, qst, 0)
+    rest(vk, qst, QC)
+    cb.wait()
+    cd.wait()
+    small(vb, qst, 2 * QC)
+    small(vd, qst, 2 * QC + 128)
+    scatter(qst, qrc, 1)
+    cv.wait()
     ups = []
     for s in range(KV):
         o = lax.rem(kv + s, KV)
@@ -142,14 +183,9 @@
         c = pltpu.make_async_copy(wu.at[rows], vu.at[rows], usem.at[s])
         c.start()
         ups.append(c)
-    cb.wait()
-    cd.wait()
-    project(vb, qst, 2 * QC)
-    project(vd, qst, 2 * QC + 128)
-    scatter(qst, qrc, 1)
-    cv.wait()
     project(vv, vst, 0)
     scatter(vst, vrc, 2)
+    cg.wait()
     downs = []
     SR = ws.shape[0] // 4
     for s in range(4):
@@ -157,7 +193,6 @@
         c = pltpu.make_async_copy(ws.at[rows], vs.at[rows], ssem.at[s])
         c.start()
         downs.append(c)
-    cg.wait()
     project(vg, gst, 0)
     scatter(gst, grc, 3)
 
@@ -184,7 +219,6 @@
     kqt = jnp.transpose(kq[...])
     value = arrive(vst, vrc, 2) * inv
     cst.wait()
-    outs = []
     for hk in range(khe):
         for s in range(own):
             i = hk * own + s
@@ -202,10 +236,6 @@
                 )
                 ho[s:s + 1, h * HEAD:(h + 1) * HEAD] = a * pq + kd * u
                 st[s, h] = a * S + kcol * u
-        hs = pl.ds(hk * rep, rep)
-        c = pltpu.make_async_copy(st.at[:, hs], new_state.at[:, hs], osem.at[hk])
-        c.start()
-        outs.append(c)
 
     gate = arrive(gst, grc, 3) * inv
     for h in range(heads):
@@ -297,16 +327,11 @@
         remote(dst.at[o], drc.at[o], d_s.at[o], d_r.at[o], o // TP, lax.rem(o, TP)).wait_recv()
         total = total + drc[o].astype(F32)
     mo[...] = total.astype(BF16)
-    last = pltpu.make_async_copy(mo, mixed, osem.at[khe])
-    last.start()
     for c in sends:
         c.wait_send()
     for s in range(1, N):
         o = lax.rem(flat + s, N)
         remote(dst.at[o], drc.at[o], d_s.at[o], d_r.at[o], o // TP, lax.rem(o, TP)).wait_send()
-    for c in outs:
-        c.wait()
-    last.wait()
 
 
 def solution(mesh):
@@ -323,16 +348,16 @@
         V = pltpu.VMEM
         S = pltpu.SemaphoreType.DMA
         args = (
-            x, g1[None], wq, wk, wv, wg, wb, wd, fexp[None], foff[None], extra, mem,
+            x, g1[None], wq, wk, wv, wg, wb.T, wd.T, fexp[None], foff[None], extra, mem,
             crs[None], wo, g2[None], wu, ws,
         )
         kqr = -(-2 * khe * own // 128) * 128
         scratch = [
             V((TP, R, C), BF16), V((TP, 1, C), F32), V((N, 1, C), F32),
             V(wq.shape, BF16), V(wk.shape, BF16), V(wv.shape, BF16), V(wg.shape, BF16),
-            V(wb.shape, BF16), V(wd.shape, BF16),
+            V(wb.shape[::-1], BF16), V(wd.shape[::-1], BF16),
             V((1, heads), F32), V((1, heads), F32), V(extra.shape, F32),
-            V(mem.shape, F32), V((1, HEAD), F32),
+            V((1, HEAD), F32),
             V(wo.shape, BF16), V(wu.shape, BF16), V(ws.shape, BF16),
             V((KV, own, 2 * QC + 256), BF16), V((KV, own, 2 * QC + 256), BF16),
             V((KV, own, VC), BF16), V((KV, own, VC), BF16),
@@ -341,8 +366,8 @@
             V((kqr, HEAD), F32), V((own, VC), F32),
             V((KV, own, VC), BF16), V((TP, R, K1), BF16), V((KV, R, K1), BF16),
             V((R, wu.shape[1]), F32), V((R, wu.shape[1]), BF16),
-            V((N, R, C), BF16), V((N, R, C), BF16), V((R, C), BF16),
-            S((15,)), S((KV,)), S((4,)), S((khe + 1,)),
+            V((N, R, C), BF16), V((N, R, C), BF16), V((R, 2 * QC), F32),
+            S((15,)), S((KV,)), S((4,)),
             S((N,)), S((N,)), S((2, TP)), S((2, TP)), S((4, KV)), S((4, KV)),
             S((KV,)), S((KV,)), S((TP,)), S((TP,)), S((KV,)), S((KV,)), S((N,)), S((N,)),
         ]
@@ -350,14 +375,14 @@
         return pl.pallas_call(
             functools.partial(layer, KV, TP, D),
             out_shape=(
-                jax.ShapeDtypeStruct((R, C), BF16),
-                jax.ShapeDtypeStruct(mem.shape, F32),
+                pltpu.VMEM((R, C), BF16),
+                pltpu.VMEM(mem.shape, F32),
             ),
             in_specs=[any_spec] * len(args),
-            out_specs=(any_spec, any_spec),
+            out_specs=(pl.BlockSpec(memory_space=pltpu.VMEM),) * 2,
             scratch_shapes=scratch,
             compiler_params=pltpu.CompilerParams(
-                collective_id=0, has_side_effects=True, vmem_limit_bytes=67043328
+                collective_id=0, has_side_effects=True, vmem_limit_bytes=VMEM_LIMIT
             ),
             name="layer",
         )(*args)

time: 43.2 us -> 35.4 us (0.82)
  local copies, waits for them, and re-layouts: 9.21 us -> 2.62 us
  Pallas kernels: 33 us -> 32 us
    unnamed x4 -> x2, local copies, waits for them, and re-layouts: 9.21 us -> 2.62 us
    pallas_call x1, Pallas kernels: 33 us -> 32 us  [on_device(): pl.pallas_call(functools.partial(layer, KV, TP, D), out_shape=(pltpu.VMEM...]
where the time goes in v2:
time: 35.4 us; the launch traced here: 35.2 us
  Pallas kernels  32 us (90%)
  local copies, waits for them, and re-layouts  2.62 us (7%)
  between operations  0.65 us (2%)
    pallas_call x1, Pallas kernels, on_device(): pl.pallas_call(functools.partial(layer, KV, TP, D), out_shape=(pltpu.VMEM...  32 us
    unnamed x2, local copies, waits for them, and re-layouts  2.62 us

profile of v2, /device:TPU:0, one launch (start us, length us, event | category | flops | bytes accessed | tf_op | source)
XLA Modules:
  0.0 35.2 jit_solution(13038143892049195403)
XLA Ops:
  0.6 32.0 %layer.1 = (bf16[16,512]{1,0:T(8,128)(2,1)S(1)}, f32[4,16,128,128]{3,2,1,0:T(8,128)S(1)}) custom-call(bf16[16,512]{1,0:T(8,128)(2,1)} %x.1, f32[1,512]{1,0:T(1,128)} %bitcast.9, bf16[1024,1024]{1,0:T(8,128)(2,1)} %wq.1, bf16[1024,1024]{1,0:T(8,128)(2,1)} %wk.1, bf16[1024,2048]{1,0:T(8,128)(2,1)} %wv.1, bf16[1024,2048]{1,0:T(8,128)(2,1)} %wg.1, ...), custom_call_target="tpu_custom_call" | custom-call | tf_op jit(solution)/shard_map/layer/pallas_call | solution.py:375
  32.6 0.6 %copy.21 = bf16[16,512]{1,0:T(8,128)(2,1)} copy(bf16[16,512]{1,0:T(8,128)(2,1)S(1)} %get-tuple-element.2) | data formatting | bytes 32768
  33.2 2.0 %copy.22 = f32[4,16,128,128]{3,2,1,0:T(8,128)} copy(f32[4,16,128,128]{3,2,1,0:T(8,128)S(1)} %get-tuple-element.3) | data formatting | bytes 8388608
